TPU v7x, 128 devices: a whole 4x4x4 slice. The times are simulated.
128 devices in a mesh: sp: 16 (over z, x), fs: 4 (over y), tp: 2 (over core).
Axes of the slice: x: 4, y: 4, z: 4, core: 2. Of those that a mesh axis runs over, the one named last changes fastest.
Arguments:
- tokens: bfloat16 [4, 8192, 2048], P('fs', 'sp', 'tp'), may hold values from -6 to 6
- norm_gain: float32 [2048], replicated, may hold values from 0.1 to 1.9
- w_pool_in: bfloat16 [2048, 512], P('fs', 'tp'), may hold values from -0.125 to 0.125
- w_query: bfloat16 [2048, 1024], P('fs', 'tp'), may hold values from -0.125 to 0.125
- w_key: bfloat16 [2048, 1024], P('fs', 'tp'), may hold values from -0.125 to 0.125
- w_value: bfloat16 [2048, 1024], P('fs', 'tp'), may hold values from -0.125 to 0.125
- query_gain: float32 [64], replicated, may hold values from 1.5 to 2.5
- key_gain: float32 [64], replicated, may hold values from 1.5 to 2.5
- stick_offset: float32 [16], P('tp'), as said below
- pool_mix: bfloat16 [4, 128, 128], P('tp'), may hold values from -0.5 to 0.5
- pool_scale: float32 [512], P('tp'), may hold values from 0.2 to 4, as said below
- pool_gain: bfloat16 [512], P('tp'), may hold values from 0.099609375 to 1.8984375
- attn_gain: bfloat16 [1024], P('tp'), may hold values from 0.099609375 to 1.8984375
- w_out_pool: bfloat16 [512, 2048], P('tp', 'fs'), may hold values from -0.15625 to 0.15625
- w_out_attn: bfloat16 [1024, 2048], P('tp', 'fs'), may hold values from -0.15625 to 0.15625
Outputs:
- mixed: bfloat16 [4, 8192, 2048], P('fs', ('sp', 'tp'))
Inputs may be any that keep to these rules, and one draw needn't show every extreme that they name: `stick_offset`: per head, negative. `pool_scale`: positive channel scales.
All inputs are finite; a program needn't handle non-finite values.
Results may differ from a plain program's by a relative error of at most 0.013.
Values may be sent and summed in bfloat16 or wider, within the bound.
A program may use at most 192 MiB of HBM per device.

v0:
```python
import math
import jax
import jax.numpy as jnp
from jax import lax
from jax.sharding import PartitionSpec as P

HEADS = 16
HEAD_DIM = 64
POOL = 512
POOL_GROUPS = 4
EPS = 1e-06


def sent_to_all(shard, axis):
    devices = lax.axis_size(axis)
    return lax.all_to_all(
        jnp.broadcast_to(shard[None], (devices, *shard.shape)), axis, 0, 0, tiled=True
    )


def in_order(parts, dim):
    lengths = list(parts.shape[1:])
    lengths[dim] *= parts.shape[0]
    return jnp.moveaxis(parts, 0, dim).reshape(lengths)


def gathered_copies(shard, axis, dim):
    parts = sent_to_all(shard, axis)
    return in_order(parts, dim)


def in_one_piece(arrays, axis, dim, along):
    both = jnp.concatenate(arrays, axis=along)
    whole, at, outs = (lax.all_gather(both, axis, axis=dim, tiled=True), 0, [])
    for a in arrays:
        outs.append(lax.slice_in_dim(whole, at, at + a.shape[along], axis=along))
        at += a.shape[along]
    return tuple(outs)


def shifted_2(value, axis, steps):
    count = lax.axis_size(axis)
    initial, last = (max(0, -steps), min(count, count - steps))
    return lax.ppermute(value, axis, [(source, source + steps) for source in range(initial, last)])


def partner_2(shard, axis, distance):
    return lax.ppermute(shard, axis, [(i, i ^ 1 << distance) for i in range(lax.axis_size(axis))])


def head_norm(projected, gain, head_count):
    split = projected.reshape(projected.shape[0], head_count, HEAD_DIM)
    factor = lax.rsqrt(jnp.mean(split * split, axis=-1, keepdims=True) + EPS)
    return (split * factor * gain).astype(jnp.bfloat16)


def stick_block(query, key_heads, value_heads, offset, carried, row_offset, score_scale):
    scores = (
        jnp.einsum("thd,khd->htk", query, key_heads, preferred_element_type=jnp.float32)
        * score_scale
        + offset[:, None, None]
    )
    keep = jax.nn.log_sigmoid(-scores)
    if row_offset is not None:
        shape = (query.shape[0], key_heads.shape[0])
        earlier = (
            lax.broadcasted_iota(jnp.int32, shape, 1)
            < lax.broadcasted_iota(jnp.int32, shape, 0) + row_offset
        )
        keep = jnp.where(earlier[None], keep, 0.0)
    running = jnp.cumsum(keep, axis=2)
    block_total = running[:, :, -1]
    log_weight = (
        jax.nn.log_sigmoid(scores) + block_total[:, :, None] - running + carried[:, :, None]
    )
    weight = jnp.exp(log_weight)
    if row_offset is not None:
        weight = jnp.where(earlier[None], weight, 0.0)
    weight = weight.astype(jnp.bfloat16)
    block_out = jnp.einsum("htk,khd->thd", weight, value_heads, preferred_element_type=jnp.float32)
    return (block_out, block_total)


def branch_norm(values_in, squares, width, gain):
    values_f = values_in.astype(jnp.float32)
    factor = lax.rsqrt(squares / width + EPS)
    return (values_f * factor[:, None] * gain.astype(jnp.float32)).astype(jnp.bfloat16)


def shards(
    tokens,
    norm_gain,
    w_pool_in,
    w_query,
    w_key,
    w_value,
    query_gain,
    key_gain,
    stick_offset,
    pool_mix,
    pool_scale,
    pool_gain,
    attn_gain,
    w_out_pool,
    w_out_attn,
):
    whole = gathered_copies(tokens, "tp", 2)[0]
    whole_f = whole.astype(jnp.float32)
    normed = (
        whole_f * lax.rsqrt(jnp.mean(whole_f * whole_f, axis=-1, keepdims=True) + EPS) * norm_gain
    ).astype(jnp.bfloat16)
    row_count = normed.shape[0]
    pieces = in_one_piece((w_pool_in, w_query, w_key, w_value), "fs", 0, 1)
    pool_raw, query_raw, key_raw, value_raw = tuple(
        (jnp.dot(normed, piece, preferred_element_type=jnp.float32) for piece in pieces)
    )
    head_count = query_raw.shape[1] // HEAD_DIM
    query = head_norm(query_raw, query_gain, head_count)
    key_heads = head_norm(key_raw, key_gain, head_count)
    value_heads = value_raw.astype(jnp.bfloat16).reshape(row_count, head_count, HEAD_DIM)
    reach = 16
    pool_in = pool_raw.astype(jnp.bfloat16)
    previous = shifted_2(pool_in[row_count - reach :], "sp", 1)
    extended = jnp.concatenate([previous, pool_in], axis=0).astype(jnp.float32)
    pool_cols = pool_in.shape[1]
    group_ch = POOL // POOL_GROUPS
    local_groups = pool_cols // group_ch
    group_ids = (
        lax.axis_index("tp") * local_groups + jnp.arange(pool_cols, dtype=jnp.int32) // group_ch
    )
    window = jnp.left_shift(jnp.int32(2), group_ids)
    summed = jnp.zeros((row_count, pool_cols), jnp.float32)
    for behind in range(reach):
        shifted = extended[reach - behind : reach - behind + row_count]
        summed = summed + jnp.where(behind < window[None, :], shifted, 0.0)
    sp_index = lax.axis_index("sp")
    position = sp_index * row_count + jnp.arange(row_count, dtype=jnp.int32)
    counted = jnp.minimum(position[:, None] + 1, window[None, :]).astype(jnp.float32)
    centered = (summed / counted - extended[reach:]).astype(jnp.bfloat16)
    pooled = jnp.einsum(
        "tgc,gcd->tgd",
        centered.reshape(row_count, local_groups, group_ch),
        pool_mix,
        preferred_element_type=jnp.float32,
    )
    pool_out = (pooled.reshape(row_count, pool_cols) * pool_scale).astype(jnp.bfloat16)
    score_scale = 1.0 / math.sqrt(HEAD_DIM)
    sp_count = lax.axis_size("sp")
    key_value = jnp.stack([key_heads, value_heads])
    everything = lax.all_gather(key_value, "sp", axis=1, tiled=True)
    half = row_count // 2
    bit_count = sp_count.bit_length() - 1

    def run_rows(query_rows, source, row_offset):
        start_carry = jnp.zeros((head_count, query_rows.shape[0]), jnp.float32)
        diagonal = lax.dynamic_slice_in_dim(everything, source * row_count, row_count, 1)
        first_out, first_carry = stick_block(
            query_rows, diagonal[0], diagonal[1], stick_offset, start_carry, row_offset, score_scale
        )

        def turn(turn_index, state):
            acc_out, acc_carry = state
            block = lax.dynamic_slice_in_dim(
                everything, (source - turn_index) * row_count, row_count, 1
            )
            block_out, block_total = stick_block(
                query_rows, block[0], block[1], stick_offset, acc_carry, None, score_scale
            )
            return (acc_out + block_out, acc_carry + block_total)

        result, unused = lax.fori_loop(1, source + 1, turn, (first_out, first_carry))
        return result.reshape(query_rows.shape[0], head_count * HEAD_DIM).astype(jnp.bfloat16)

    guest_query = query[half:]
    for bit in range(bit_count):
        guest_query = partner_2(guest_query, "sp", bit)
    partner = sp_count - 1 - sp_index
    own_rows = run_rows(query[:half], sp_index, 0)
    guest_rows = run_rows(guest_query, partner, half)
    for bit in range(bit_count):
        guest_rows = partner_2(guest_rows, "sp", bit)
    attn_out = jnp.concatenate([own_rows, guest_rows], axis=0)
    w_pool_cols, w_attn_cols = (
        lax.all_gather(w_out_pool, "fs", axis=1, tiled=True),
        lax.all_gather(w_out_attn, "fs", axis=1, tiled=True),
    )
    pool_rows, attn_rows = (
        lax.all_to_all(pool_out, "tp", split_axis=0, concat_axis=1, tiled=True),
        lax.all_to_all(attn_out, "tp", split_axis=0, concat_axis=1, tiled=True),
    )
    w_pool_all, w_attn_all, pool_gain_all, attn_gain_all = (
        lax.all_gather(w_pool_cols, "tp", axis=0, tiled=True),
        lax.all_gather(w_attn_cols, "tp", axis=0, tiled=True),
        lax.all_gather(pool_gain, "tp", axis=0, tiled=True),
        lax.all_gather(attn_gain, "tp", axis=0, tiled=True),
    )
    pool_f = pool_rows.astype(jnp.float32)
    attn_f = attn_rows.astype(jnp.float32)
    pool_normed = branch_norm(pool_rows, jnp.sum(pool_f * pool_f, axis=-1), POOL, pool_gain_all)
    attn_normed = branch_norm(
        attn_rows, jnp.sum(attn_f * attn_f, axis=-1), HEADS * HEAD_DIM, attn_gain_all
    )
    mixed = jnp.dot(pool_normed, w_pool_all, preferred_element_type=jnp.float32) + jnp.dot(
        attn_normed, w_attn_all, preferred_element_type=jnp.float32
    )
    return mixed.astype(jnp.bfloat16)[None]


def solution(mesh):
    in_specs = (
        P("fs", "sp", "tp"),
        P(),
        P("fs", "tp"),
        P("fs", "tp"),
        P("fs", "tp"),
        P("fs", "tp"),
        P(),
        P(),
        P("tp"),
        P("tp", None, None),
        P("tp"),
        P("tp"),
        P("tp"),
        P("tp", "fs"),
        P("tp", "fs"),
    )
    out_specs = P("fs", ("sp", "tp"), None)
    return jax.shard_map(shards, mesh=mesh, in_specs=in_specs, out_specs=out_specs, check_vma=False)
```

profile of v0, /device:TPU:103, one launch (start us, length us, event | category | flops | bytes accessed | tf_op | source)
XLA Modules:
  0.0 761.2 jit_solution(1497514801564157925)
XLA Ops:
  11.9 5.5 all-to-all-start
  27.3 57.7 %all-gather.9.cloned.1.call-done = bf16[2048,1792]{1,0:T(8,128)(2,1)} async-done(((bf16[512,1792]{1,0:T(8,128)(2,1)}), bf16[2048,1792]{1,0:T(8,128)(2,1)}) %all-gather.9.cloned.1.call-update) | async-done | bytes 7340048 | tf_op jit(solution)/shard_map/all_gather | solution.py:34
  101.0 17.3 %all-gather.17.cloned.1.call-done = bf16[512,2048]{1,0:T(8,128)(2,1)} async-done(((bf16[512,512]{1,0:T(8,128)(2,1)}), bf16[512,2048]{1,0:T(8,128)(2,1)}) %all-gather.17.cloned.1.call-update) | async-done | bytes 2097168 | tf_op jit(solution)/shard_map/all_gather | solution.py:185
  134.2 8.0 %all-gather.11.cloned.1.call-done = bf16[256,2048]{1,0:T(8,128)(2,1)} async-done(((bf16[256,512]{1,0:T(8,128)(2,1)}), bf16[256,2048]{1,0:T(8,128)(2,1)}) %all-gather.11.cloned.1.call-update) | async-done | bytes 1048592 | tf_op jit(solution)/shard_map/all_gather | solution.py:184
  146.6 6.6 all-to-all-start.1
  154.5 8.8 %collective-permute-done.3 = bf16[256,8,64]{0,2,1:T(8,128)(2,1)S(1)} collective-permute-done((bf16[256,8,64]{0,2,1:T(8,128)(2,1)S(1)}, bf16[256,8,64]{0,2,1:T(8,128)(2,1)S(1)}, u32[]{:S(2)}, u32[]{:S(2)}) %collective-permute-start.3) | collective-permute-done | bytes 262176 | tf_op jit(solution)/shard_map/ppermute | solution.py:48
  165.4 5.4 collective-permute-done.4
  170.8 97.9 %all-gather.15.cloned.1.call-done = bf16[2,8192,8,64]{1,3,2,0:T(8,128)(2,1)} async-done(((bf16[2,512,8,64]{1,3,2,0:T(8,128)(2,1)}), bf16[2,8192,8,64]{1,3,2,0:T(8,128)(2,1)}) %all-gather.15.cloned.1.call-update) | async-done | bytes 16777232 | tf_op jit(solution)/shard_map/all_gather | solution.py:150
  270.6 10.6 %fusion.63 = (f32[8,256,512]{2,1,0:T(8,128)}, f32[8,256,512]{2,1,0:T(8,128)}, f32[8,256,512]{2,1,0:T(8,128)}) fusion(f32[8]{0:T(128)S(1)} %copy-done.14, pred[256,512]{1,0:T(8,128)(4,1)S(1)} %get-tuple-element.157, f32[8,256,512]{2,1,0:T(8,128)S(1)} %fusion.97, pred[256,512]{1,0:T(8,128)(4,1)S(1)} %get-tuple-element.156, ...), kind=kOutput, calls=%fused_computation.79 | convolution fusion | flops 155189248 | bytes 17826308 | tf_op jit(solution)/shard_map/thd,khd->htk/dot_general | solution.py:59
  281.2 5.7 copy.122
  286.9 5.6 copy.124
  297.5 5.3 copy.125
  304.8 6.4 fusion.88
  311.4 14.4 %collective-permute-start.5 = (bf16[256,512]{0,1:T(8,128)(2,1)S(1)}, bf16[256,512]{0,1:T(8,128)(2,1)S(1)}, u32[]{:S(2)}, u32[]{:S(2)}) collective-permute-start(bf16[256,512]{0,1:T(8,128)(2,1)S(1)} %bitcast.254), channel_id=1, source_target_pairs={{0,8},{8,0},{16,24},{24,16},{32,40},{40,32},{48,56},{56,48},{64,72... | collective-permute-start | bytes 786440 | tf_op jit(solution)/shard_map/ppermute | solution.py:48
  330.5 28.5 %collective-permute-start.6 = (bf16[256,512]{0,1:T(8,128)(2,1)S(1)}, bf16[256,512]{0,1:T(8,128)(2,1)S(1)}, u32[]{:S(2)}, u32[]{:S(2)}) collective-permute-start(bf16[256,512]{0,1:T(8,128)(2,1)S(1)} %collective-permute-done.5), channel_id=1, source_target_pairs={{0,16},{8,24},{16,0},{24,8},{32,48},{40,56},{48,32},{56,40},{64,80... | collective-permute-start | bytes 786440 | tf_op jit(solution)/shard_map/ppermute | solution.py:48
  361.2 5.3 copy.123
  368.3 53.3 %collective-permute-start.7 = (bf16[256,512]{0,1:T(8,128)(2,1)S(1)}, bf16[256,512]{0,1:T(8,128)(2,1)S(1)}, u32[]{:S(2)}, u32[]{:S(2)}) collective-permute-start(bf16[256,512]{0,1:T(8,128)(2,1)S(1)} %collective-permute-done.6), channel_id=1, source_target_pairs={{0,32},{8,40},{16,48},{24,56},{32,0},{40,8},{48,16},{56,24},{64,96... | collective-permute-start | bytes 786440 | tf_op jit(solution)/shard_map/ppermute | solution.py:48
  421.7 6.4 fusion.85
  428.1 110.3 %collective-permute-start.8 = (bf16[256,512]{0,1:T(8,128)(2,1)S(1)}, bf16[256,512]{0,1:T(8,128)(2,1)S(1)}, u32[]{:S(2)}, u32[]{:S(2)}) collective-permute-start(bf16[256,512]{0,1:T(8,128)(2,1)S(1)} %collective-permute-done.7), channel_id=1, source_target_pairs={{0,64},{8,72},{16,80},{24,88},{32,96},{40,104},{48,112},{56,120},{... | collective-permute-start | bytes 786440 | tf_op jit(solution)/shard_map/ppermute | solution.py:48
  538.4 200.5 %while.24 = (s32[]{:T(128)}, f32[256,8,64]{0,2,1:T(8,128)S(1)}, f32[8,256]{1,0:T(8,128)S(1)}, s32[]{:T(128)}, s32[]{:T(128)}, /*index=5*/bf16[2,8192,8,64]{1,3,2...) while((s32[]{:T(128)}, f32[256,8,64]{0,2,1:T(8,128)S(1)}, ...), condition=%wide.region_9.10_spmd, body=%wide.region_6.9_spmd.sunk | while | flops 426934272 | bytes 44548372 | solution.py:171
  547.0 4.7 fusion.179
  573.7 4.7 fusion.179
  600.5 4.7 fusion.179
  739.3 6.9 all_to_all.28
  (278 shorter events, 265.0 us)
Async XLA Ops:
  6.5 137.0 %copy-start = (bf16[2,128,128]{2,1,0:T(8,128)(2,1)S(1)}, bf16[2,128,128]{2,1,0:T(8,128)(2,1)}, u32[]{:S(2)}) copy-start(bf16[2,128,128]{2,1,0:T(8,128)(2,1)} %param.28) | copy-start | bytes 196612
  6.5 78.5 %all-gather.9.cloned.1.call-start = ((), (), s32[]{:S(2)}) async-start(), calls=%async_computation.3 | async-start | bytes 9175040 | tf_op jit(solution)/shard_map/all_gather | solution.py:34
  9.5 8.7 %copy-start.7 = (f32[2048]{0:T(1024)S(1)}, f32[2048]{0:T(1024)}, u32[]{:S(2)}) copy-start(f32[2048]{0:T(1024)} %param.20) | copy-start | bytes 24580
  9.5 108.8 %all-gather.17.cloned.1.call-start = ((), (), s32[]{:S(2)}) async-start(), calls=%async_computation.7 | async-start | bytes 2621440 | tf_op jit(solution)/shard_map/all_gather | solution.py:185
  11.9 8.1 %all-to-all-start = ((bf16[2,1,512,1024]{3,2,1,0:T(8,128)(2,1)}), bf16[2,1,512,1024]{3,2,1,0:T(8,128)(2,1)}, u32[]{:S(2)}, u32[]{:S(2)}) async-start(bf16[2,1,512,1024]{3,2,1,0:T(8,128)(2,1)} %broadcast_in_dim.182), calls=%async_computation | async-start | bytes 4194304 | tf_op jit(solution)/shard_map/all_to_all | solution.py:16
  17.4 124.8 %all-gather.11.cloned.1.call-start = ((), (), s32[]{:S(2)}) async-start(), calls=%async_computation.4 | async-start | bytes 1310720 | tf_op jit(solution)/shard_map/all_gather | solution.py:184
  18.1 250.7 %all-gather.15.cloned.1.call-start = ((), (), s32[]{:S(2)}) async-start(), calls=%async_computation.6 | async-start | bytes 17825792 | tf_op jit(solution)/shard_map/all_gather | solution.py:150
  100.9 646.2 %all-gather.19.cloned.1.call-start = ((), (), s32[]{:S(2)}) async-start(), calls=%async_computation.8 | async-start | bytes 6291456 | tf_op jit(solution)/shard_map/all_gather | solution.py:193
  118.3 632.3 %all-gather.13.cloned.1.call-start = ((), (), s32[]{:S(2)}) async-start(), calls=%async_computation.5 | async-start | bytes 3145728 | tf_op jit(solution)/shard_map/all_gather | solution.py:192
  124.9 6.9 copy-start.10
  125.2 17.1 %collective-permute-start.1 = (bf16[256,8,64]{0,2,1:T(8,128)(2,1)S(1)}, bf16[256,8,64]{0,2,1:T(8,128)(2,1)S(1)}, u32[]{:S(2)}, u32[]{:S(2)}) collective-permute-start(bf16[256,8,64]{0,2,1:T(8,128)(2,1)S(1)} %get-tuple-element.132), channel_id=1, source_target_pairs={{0,8},{8,0},{16,24},{24,16},{32,40},{40,32},{48,56},{56,48},{64,72... | collective-permute-start | bytes 786440 | tf_op jit(solution)/shard_map/ppermute | solution.py:48
  127.9 14.4 %collective-permute-start = (bf16[16,256]{1,0:T(8,128)(2,1)S(1)}, bf16[16,256]{1,0:T(8,128)(2,1)S(1)}, u32[]{:S(2)}, u32[]{:S(2)}) collective-permute-start(bf16[16,256]{1,0:T(8,128)(2,1)S(1)} %slice.170), channel_id=1, source_target_pairs={{0,8},{8,16},{16,24},{24,32},{32,40},{40,48},{48,56},{56,64},{64,7... | collective-permute-start | bytes 24584 | tf_op jit(solution)/shard_map/ppermute | solution.py:44
  142.3 10.9 %collective-permute-start.2 = (bf16[256,8,64]{0,2,1:T(8,128)(2,1)S(1)}, bf16[256,8,64]{0,2,1:T(8,128)(2,1)S(1)}, u32[]{:S(2)}, u32[]{:S(2)}) collective-permute-start(bf16[256,8,64]{0,2,1:T(8,128)(2,1)S(1)} %collective-permute-done.1), channel_id=1, source_target_pairs={{0,16},{8,24},{16,0},{24,8},{32,48},{40,56},{48,32},{56,40},{64,80... | collective-permute-start | bytes 786440 | tf_op jit(solution)/shard_map/ppermute | solution.py:48
  146.6 124.0 %copy-start.14 = (f32[8]{0:T(128)S(1)}, f32[8]{0:T(128)}, u32[]{:S(2)}) copy-start(f32[8]{0:T(128)} %param.27) | copy-start | bytes 100
  146.6 7.8 %all-to-all-start.1 = ((bf16[2,256,256]{2,1,0:T(8,128)(2,1)}), bf16[2,256,256]{2,1,0:T(8,128)(2,1)S(1)}, u32[]{:S(2)}, u32[]{:S(2)}) async-start(bf16[2,256,256]{2,1,0:T(8,128)(2,1)} %multiply_convert_fusion.3), calls=%async_computation.1 | async-start | bytes 524288 | tf_op jit(solution)/shard_map/all_to_all | solution.py:188
  153.2 10.2 %collective-permute-start.3 = (bf16[256,8,64]{0,2,1:T(8,128)(2,1)S(1)}, bf16[256,8,64]{0,2,1:T(8,128)(2,1)S(1)}, u32[]{:S(2)}, u32[]{:S(2)}) collective-permute-start(bf16[256,8,64]{0,2,1:T(8,128)(2,1)S(1)} %collective-permute-done.2), channel_id=1, source_target_pairs={{0,32},{8,40},{16,48},{24,56},{32,0},{40,8},{48,16},{56,24},{64,96... | collective-permute-start | bytes 786440 | tf_op jit(solution)/shard_map/ppermute | solution.py:48
  163.3 7.5 collective-permute-start.4
  270.6 10.6 %copy-start.2 = (f32[8,256,512]{2,1,0:T(8,128)}, f32[8,256,512]{2,1,0:T(8,128)S(1)}, u32[]{:S(2)}) copy-start(f32[8,256,512]{2,1,0:T(8,128)S(1)} %fusion.97) | copy-start | bytes 12582916
  311.4 19.1 %collective-permute-start.5 = (bf16[256,512]{0,1:T(8,128)(2,1)S(1)}, bf16[256,512]{0,1:T(8,128)(2,1)S(1)}, u32[]{:S(2)}, u32[]{:S(2)}) collective-permute-start(bf16[256,512]{0,1:T(8,128)(2,1)S(1)} %bitcast.254), channel_id=1, source_target_pairs={{0,8},{8,0},{16,24},{24,16},{32,40},{40,32},{48,56},{56,48},{64,72... | collective-permute-start | bytes 786440 | tf_op jit(solution)/shard_map/ppermute | solution.py:48
  330.5 37.8 %collective-permute-start.6 = (bf16[256,512]{0,1:T(8,128)(2,1)S(1)}, bf16[256,512]{0,1:T(8,128)(2,1)S(1)}, u32[]{:S(2)}, u32[]{:S(2)}) collective-permute-start(bf16[256,512]{0,1:T(8,128)(2,1)S(1)} %collective-permute-done.5), channel_id=1, source_target_pairs={{0,16},{8,24},{16,0},{24,8},{32,48},{40,56},{48,32},{56,40},{64,80... | collective-permute-start | bytes 786440 | tf_op jit(solution)/shard_map/ppermute | solution.py:48
  368.3 59.7 %collective-permute-start.7 = (bf16[256,512]{0,1:T(8,128)(2,1)S(1)}, bf16[256,512]{0,1:T(8,128)(2,1)S(1)}, u32[]{:S(2)}, u32[]{:S(2)}) collective-permute-start(bf16[256,512]{0,1:T(8,128)(2,1)S(1)} %collective-permute-done.6), channel_id=1, source_target_pairs={{0,32},{8,40},{16,48},{24,56},{32,0},{40,8},{48,16},{56,24},{64,96... | collective-permute-start | bytes 786440 | tf_op jit(solution)/shard_map/ppermute | solution.py:48
  428.1 310.9 %collective-permute-start.8 = (bf16[256,512]{0,1:T(8,128)(2,1)S(1)}, bf16[256,512]{0,1:T(8,128)(2,1)S(1)}, u32[]{:S(2)}, u32[]{:S(2)}) collective-permute-start(bf16[256,512]{0,1:T(8,128)(2,1)S(1)} %collective-permute-done.7), channel_id=1, source_target_pairs={{0,64},{8,72},{16,80},{24,88},{32,96},{40,104},{48,112},{56,120},{... | collective-permute-start | bytes 786440 | tf_op jit(solution)/shard_map/ppermute | solution.py:48
  738.9 7.9 %copy-start.8 = (f32[2,1,512]{2,1,0:T(1,128)S(1)}, f32[2,1,512]{2,1,0:T(1,128)}, u32[]{:S(2)}) copy-start(f32[2,1,512]{2,1,0:T(1,128)} %convert_element_type.154) | copy-start | bytes 12292
  747.1 6.8 copy-start.1
  (8 other events, 29.9 us)
Sparse Core Ops, SparseCore 0:
  9.6 75.4 all-gather.8
  86.7 31.5 all-gather.16
  120.0 22.1 all-gather.10
  144.2 124.5 all-gather.14
  270.3 19.9 all-gather.18
  291.7 14.6 all-gather.12
where the time goes:
time: 772 us; the launch traced here: 761 us
  starting transfers between devices  224 us (29%)
  waiting for transfers between devices  201 us (26%)
  matrix products  178 us (23%)
  other arithmetic  68 us (9%)
  local copies, waits for them, and re-layouts  63.1 us (8%)
  between operations  14.4 us (2%)
  blocking collectives  11.4 us (1%)
    ppermute x8, starting transfers between devices, partner_2(): lax.ppermute(shard, axis, [(i, i ^ 1 << distance) for i in range(lax.axis...  210 us
    all_gather x1, waiting for transfers between devices, shards(): everything = lax.all_gather(key_value, 'sp', axis=1, tiled=True)  97.9 us
    dot_general x17, matrix products, stick_block(): jnp.einsum('htk,khd->thd', weight, value_heads, preferred_element_type=jn...  84 us
    dot_general x17, matrix products, stick_block(): jnp.einsum('thd,khd->htk', query, key_heads, preferred_element_type=jnp.f...  73.4 us
    another operation x52, other arithmetic  57.9 us
    all_gather x1, waiting for transfers between devices, in_one_piece(): whole, at, outs = (lax.all_gather(both, axis, axis=dim, tiled=True), 0, [])  57.7 us
    another operation x36, local copies, waits for them, and re-layouts  42.3 us
    all_gather x1, waiting for transfers between devices, shards(): lax.all_gather(w_out_attn, 'fs', axis=1, tiled=True)  17.3 us
  transfers between devices with their start and end apart: 17, of which 9 were waited for; matrix products, arithmetic and copies ran while one was open for 40% of the time, Pallas kernels for 0%

commit v1 on v0

--- a/solution.py
+++ b/solution.py
@@ -147,7 +147,10 @@
     score_scale = 1.0 / math.sqrt(HEAD_DIM)
     sp_count = lax.axis_size("sp")
     key_value = jnp.stack([key_heads, value_heads])
-    everything = lax.all_gather(key_value, "sp", axis=1, tiled=True)
+    size = lax.axis_size("sp")
+    tiles = jnp.stack([key_value for _ in range(size)])
+    tiles = lax.all_to_all(tiles, "sp", split_axis=0, concat_axis=0)
+    everything = jnp.concatenate(tiles, axis=1)
     half = row_count // 2
     bit_count = sp_count.bit_length() - 1
 

time: 772 us -> 908 us (1.18)
  waiting for transfers between devices: 201 us -> 314 us
  local copies, waits for them, and re-layouts: 63.1 us -> 79.7 us
  blocking collectives: 11.4 us -> 21.3 us
    ppermute x8, waiting for transfers between devices: 16.3 us -> 219 us  [partner_2(): lax.ppermute(shard, axis, [(i, i ^ 1 << distance) for i in range(lax.axis...]
    all_gather x1 -> x0, waiting for transfers between devices: 97.9 us -> none  [shards(): everything = lax.all_gather(key_value, 'sp', axis=1, tiled=True)]
    all_gather x1, waiting for transfers between devices: 17.3 us -> 32.7 us  [shards(): lax.all_gather(w_out_attn, 'fs', axis=1, tiled=True)]
    another operation x36 -> x37, local copies, waits for them, and re-layouts: 42.3 us -> 47.8 us
  transfers between devices with their start and end apart: 17 -> 16, of which waited for: 9 -> 7; matrix products, arithmetic and copies ran while one was open for 40% -> 33% of each run, Pallas kernels for 0% -> 0%
where the time goes in v1:
time: 908 us; the launch traced here: 897 us
  waiting for transfers between devices  314 us (35%)
  starting transfers between devices  222 us (24%)
  matrix products  176 us (19%)
  local copies, waits for them, and re-layouts  79.7 us (9%)
  other arithmetic  67.5 us (7%)
  blocking collectives  21.3 us (2%)
  between operations  14.1 us (2%)
    ppermute x8, waiting for transfers between devices, partner_2(): lax.ppermute(shard, axis, [(i, i ^ 1 << distance) for i in range(lax.axis...  219 us
    ppermute x8, starting transfers between devices, partner_2(): lax.ppermute(shard, axis, [(i, i ^ 1 << distance) for i in range(lax.axis...  208 us
    dot_general x17, matrix products, stick_block(): jnp.einsum('htk,khd->thd', weight, value_heads, preferred_element_type=jn...  84 us
    dot_general x17, matrix products, stick_block(): jnp.einsum('thd,khd->htk', query, key_heads, preferred_element_type=jnp.f...  71.8 us
    all_gather x1, waiting for transfers between devices, in_one_piece(): whole, at, outs = (lax.all_gather(both, axis, axis=dim, tiled=True), 0, [])  58.3 us
    another operation x52, other arithmetic  57.8 us
    another operation x36, local copies, waits for them, and re-layouts  41.9 us
    all_gather x1, waiting for transfers between devices, shards(): lax.all_gather(w_out_attn, 'fs', axis=1, tiled=True)  32.7 us
  transfers between devices with their start and end apart: 16, of which 7 were waited for; matrix products, arithmetic and copies ran while one was open for 33% of the time, Pallas kernels for 0%

profile of v1, /device:TPU:103, one launch (start us, length us, event | category | flops | bytes accessed | tf_op | source)
XLA Modules:
  0.0 896.5 jit_solution(2354935361996138953)
XLA Ops:
  11.1 5.5 all-to-all-start
  26.8 58.3 %all-gather.8.cloned.1.call-done = bf16[2048,1792]{1,0:T(8,128)(2,1)} async-done(((bf16[512,1792]{1,0:T(8,128)(2,1)}), bf16[2048,1792]{1,0:T(8,128)(2,1)}) %all-gather.8.cloned.1.call-update) | async-done | bytes 7340048 | tf_op jit(solution)/shard_map/all_gather | solution.py:34
  109.1 5.4 all_to_all.33
  114.5 6.0 stack.8
  120.5 7.4 all-to-all-start.2
  129.4 32.7 %all-gather.14.cloned.1.call-done = bf16[512,2048]{1,0:T(8,128)(2,1)} async-done(((bf16[512,512]{1,0:T(8,128)(2,1)}), bf16[512,2048]{1,0:T(8,128)(2,1)}) %all-gather.14.cloned.1.call-update) | async-done | bytes 2097168 | tf_op jit(solution)/shard_map/all_gather | solution.py:188
  169.2 210.3 %collective-permute-done.1 = bf16[256,8,64]{0,2,1:T(8,128)(2,1)S(1)} collective-permute-done((bf16[256,8,64]{0,2,1:T(8,128)(2,1)S(1)}, bf16[256,8,64]{0,2,1:T(8,128)(2,1)S(1)}, u32[]{:S(2)}, u32[]{:S(2)}) %collective-permute-start.1) | collective-permute-done | bytes 262176 | tf_op jit(solution)/shard_map/ppermute | solution.py:48
  388.1 5.4 collective-permute-done.3
  396.1 8.8 copy.131
  405.7 10.0 %fusion.63 = (f32[8,256,512]{2,1,0:T(8,128)}, f32[8,256,512]{2,1,0:T(8,128)}, f32[8,256,512]{2,1,0:T(8,128)}) fusion(f32[8]{0:T(128)S(1)} %copy-done.14, pred[256,512]{1,0:T(8,128)(4,1)S(1)} %get-tuple-element.157, f32[8,256,512]{2,1,0:T(8,128)S(1)} %fusion.97, pred[256,512]{1,0:T(8,128)(4,1)S(1)} %get-tuple-element.156, ...), kind=kOutput, calls=%fused_computation.79 | convolution fusion | flops 155189248 | bytes 17826308 | tf_op jit(solution)/shard_map/thd,khd->htk/dot_general | solution.py:59
  415.7 5.5 copy.124
  421.2 5.5 copy.126
  431.6 5.3 copy.127
  438.7 6.4 fusion.88
  445.4 12.7 %collective-permute-start.5 = (bf16[256,512]{0,1:T(8,128)(2,1)S(1)}, bf16[256,512]{0,1:T(8,128)(2,1)S(1)}, u32[]{:S(2)}, u32[]{:S(2)}) collective-permute-start(bf16[256,512]{0,1:T(8,128)(2,1)S(1)} %bitcast.261), channel_id=1, source_target_pairs={{0,8},{8,0},{16,24},{24,16},{32,40},{40,32},{48,56},{56,48},{64,72... | collective-permute-start | bytes 786440 | tf_op jit(solution)/shard_map/ppermute | solution.py:48
  461.9 29.6 %collective-permute-start.6 = (bf16[256,512]{0,1:T(8,128)(2,1)S(1)}, bf16[256,512]{0,1:T(8,128)(2,1)S(1)}, u32[]{:S(2)}, u32[]{:S(2)}) collective-permute-start(bf16[256,512]{0,1:T(8,128)(2,1)S(1)} %collective-permute-done.5), channel_id=1, source_target_pairs={{0,16},{8,24},{16,0},{24,8},{32,48},{40,56},{48,32},{56,40},{64,80... | collective-permute-start | bytes 786440 | tf_op jit(solution)/shard_map/ppermute | solution.py:48
  493.8 5.3 copy.125
  500.9 52.9 %collective-permute-start.7 = (bf16[256,512]{0,1:T(8,128)(2,1)S(1)}, bf16[256,512]{0,1:T(8,128)(2,1)S(1)}, u32[]{:S(2)}, u32[]{:S(2)}) collective-permute-start(bf16[256,512]{0,1:T(8,128)(2,1)S(1)} %collective-permute-done.6), channel_id=1, source_target_pairs={{0,32},{8,40},{16,48},{24,56},{32,0},{40,8},{48,16},{56,24},{64,96... | collective-permute-start | bytes 786440 | tf_op jit(solution)/shard_map/ppermute | solution.py:48
  553.9 6.4 fusion.85
  560.3 109.6 %collective-permute-start.8 = (bf16[256,512]{0,1:T(8,128)(2,1)S(1)}, bf16[256,512]{0,1:T(8,128)(2,1)S(1)}, u32[]{:S(2)}, u32[]{:S(2)}) collective-permute-start(bf16[256,512]{0,1:T(8,128)(2,1)S(1)} %collective-permute-done.7), channel_id=1, source_target_pairs={{0,64},{8,72},{16,80},{24,88},{32,96},{40,104},{48,112},{56,120},{... | collective-permute-start | bytes 786440 | tf_op jit(solution)/shard_map/ppermute | solution.py:48
  669.9 200.5 %while.24 = (s32[]{:T(128)}, f32[256,8,64]{0,2,1:T(8,128)S(1)}, f32[8,256]{1,0:T(8,128)S(1)}, s32[]{:T(128)}, s32[]{:T(128)}, /*index=5*/bf16[2,8192,8,64]{1,3,2...) while((s32[]{:T(128)}, f32[256,8,64]{0,2,1:T(8,128)S(1)}, ...), condition=%wide.region_9.10_spmd, body=%wide.region_6.9_spmd.sunk | while | flops 426934272 | bytes 44548372 | solution.py:174
  691.9 4.7 fusion.179
  732.0 4.7 fusion.179
  870.7 11.2 %all_to_all.34 = bf16[2,256,512]{2,1,0:T(8,128)(2,1)S(1)} all-to-all(bf16[2,256,512]{2,1,0:T(8,128)(2,1)S(1)} %bitcast.255), channel_id=1, replica_groups=mesh['sp'=16,'fs'=4,'tp'=2] {'tp'}, dimensions={0} | all-to-all | bytes 1048576 | tf_op jit(solution)/shard_map/all_to_all | solution.py:192
  (278 shorter events, 271.2 us)
Async XLA Ops:
  6.5 96.6 %copy-start = (bf16[2,128,128]{2,1,0:T(8,128)(2,1)S(1)}, bf16[2,128,128]{2,1,0:T(8,128)(2,1)}, u32[]{:S(2)}) copy-start(bf16[2,128,128]{2,1,0:T(8,128)(2,1)} %param.28) | copy-start | bytes 196612
  6.5 78.6 %all-gather.8.cloned.1.call-start = ((), (), s32[]{:S(2)}) async-start(), calls=%async_computation.4 | async-start | bytes 9175040 | tf_op jit(solution)/shard_map/all_gather | solution.py:34
  9.5 7.2 copy-start.7
  11.1 8.2 all-to-all-start
  98.5 4.5 collective-permute-start
  120.5 275.6 %all-to-all-start.2 = ((bf16[16,2,512,8,64]{2,4,3,1,0:T(8,128)(2,1)}), bf16[16,2,512,8,64]{2,4,3,1,0:T(8,128)(2,1)}, u32[]{:S(2)}, u32[]{:S(2)}) async-start(bf16[16,2,512,8,64]{2,4,3,1,0:T(8,128)(2,1)} %stack.8), calls=%async_computation.2 | async-start | bytes 33554432 | tf_op jit(solution)/shard_map/all_to_all | solution.py:152
  127.9 34.3 %all-gather.14.cloned.1.call-start = ((), (), s32[]{:S(2)}) async-start(), calls=%async_computation.7 | async-start | bytes 2621440 | tf_op jit(solution)/shard_map/all_gather | solution.py:188
  128.6 257.0 %all-gather.10.cloned.1.call-start = ((), (), s32[]{:S(2)}) async-start(), calls=%async_computation.5 | async-start | bytes 1310720 | tf_op jit(solution)/shard_map/all_gather | solution.py:187
  129.4 753.4 %all-gather.16.cloned.1.call-start = ((), (), s32[]{:S(2)}) async-start(), calls=%async_computation.8 | async-start | bytes 6291456 | tf_op jit(solution)/shard_map/all_gather | solution.py:196
  162.2 724.2 %all-gather.12.cloned.1.call-start = ((), (), s32[]{:S(2)}) async-start(), calls=%async_computation.6 | async-start | bytes 3145728 | tf_op jit(solution)/shard_map/all_gather | solution.py:195
  164.7 215.3 %copy-start.13 = (bf16[256]{0:T(256)(128)(2,1)S(1)}, bf16[256]{0:T(256)(128)(2,1)}, u32[]{:S(2)}) copy-start(bf16[256]{0:T(256)(128)(2,1)} %param.30) | copy-start | bytes 1540
  164.7 218.2 %copy-start.10 = (bf16[512]{0:T(512)(128)(2,1)S(1)}, bf16[512]{0:T(512)(128)(2,1)}, u32[]{:S(2)}) copy-start(bf16[512]{0:T(512)(128)(2,1)} %param.31) | copy-start | bytes 3076
  168.5 211.0 %collective-permute-start.1 = (bf16[256,8,64]{0,2,1:T(8,128)(2,1)S(1)}, bf16[256,8,64]{0,2,1:T(8,128)(2,1)S(1)}, u32[]{:S(2)}, u32[]{:S(2)}) collective-permute-start(bf16[256,8,64]{0,2,1:T(8,128)(2,1)S(1)} %get-tuple-element.132), channel_id=1, source_target_pairs={{0,8},{8,0},{16,24},{24,16},{32,40},{40,32},{48,56},{56,48},{64,72... | collective-permute-start | bytes 786440 | tf_op jit(solution)/shard_map/ppermute | solution.py:48
  379.5 8.4 collective-permute-start.2
  387.9 5.6 collective-permute-start.3
  393.4 11.5 %collective-permute-start.4 = (bf16[256,8,64]{0,2,1:T(8,128)(2,1)S(1)}, bf16[256,8,64]{0,2,1:T(8,128)(2,1)S(1)}, u32[]{:S(2)}, u32[]{:S(2)}) collective-permute-start(bf16[256,8,64]{0,2,1:T(8,128)(2,1)S(1)} %collective-permute-done.3), channel_id=1, source_target_pairs={{0,64},{8,72},{16,80},{24,88},{32,96},{40,104},{48,112},{56,120},{... | collective-permute-start | bytes 786440 | tf_op jit(solution)/shard_map/ppermute | solution.py:48
  404.9 10.8 %copy-start.2 = (bf16[16,2,8,8,8,512]{5,4,0,3,2,1:T(8,128)(2,1)}, bf16[16,2,8,8,8,512]{5,4,0,3,2,1:T(8,128)(2,1)S(1)}, u32[]{:S(2)}) copy-start(bf16[16,2,8,8,8,512]{5,4,0,3,2,1:T(8,128)(2,1)S(1)} %copy.131) | copy-start | bytes 50331652
  405.7 10.1 %copy-start.3 = (f32[8,256,512]{2,1,0:T(8,128)}, f32[8,256,512]{2,1,0:T(8,128)S(1)}, u32[]{:S(2)}) copy-start(f32[8,256,512]{2,1,0:T(8,128)S(1)} %fusion.97) | copy-start | bytes 12582916
  445.4 16.5 %collective-permute-start.5 = (bf16[256,512]{0,1:T(8,128)(2,1)S(1)}, bf16[256,512]{0,1:T(8,128)(2,1)S(1)}, u32[]{:S(2)}, u32[]{:S(2)}) collective-permute-start(bf16[256,512]{0,1:T(8,128)(2,1)S(1)} %bitcast.261), channel_id=1, source_target_pairs={{0,8},{8,0},{16,24},{24,16},{32,40},{40,32},{48,56},{56,48},{64,72... | collective-permute-start | bytes 786440 | tf_op jit(solution)/shard_map/ppermute | solution.py:48
  461.9 39.0 %collective-permute-start.6 = (bf16[256,512]{0,1:T(8,128)(2,1)S(1)}, bf16[256,512]{0,1:T(8,128)(2,1)S(1)}, u32[]{:S(2)}, u32[]{:S(2)}) collective-permute-start(bf16[256,512]{0,1:T(8,128)(2,1)S(1)} %collective-permute-done.5), channel_id=1, source_target_pairs={{0,16},{8,24},{16,0},{24,8},{32,48},{40,56},{48,32},{56,40},{64,80... | collective-permute-start | bytes 786440 | tf_op jit(solution)/shard_map/ppermute | solution.py:48
  500.9 59.4 %collective-permute-start.7 = (bf16[256,512]{0,1:T(8,128)(2,1)S(1)}, bf16[256,512]{0,1:T(8,128)(2,1)S(1)}, u32[]{:S(2)}, u32[]{:S(2)}) collective-permute-start(bf16[256,512]{0,1:T(8,128)(2,1)S(1)} %collective-permute-done.6), channel_id=1, source_target_pairs={{0,32},{8,40},{16,48},{24,56},{32,0},{40,8},{48,16},{56,24},{64,96... | collective-permute-start | bytes 786440 | tf_op jit(solution)/shard_map/ppermute | solution.py:48
  560.3 310.2 %collective-permute-start.8 = (bf16[256,512]{0,1:T(8,128)(2,1)S(1)}, bf16[256,512]{0,1:T(8,128)(2,1)S(1)}, u32[]{:S(2)}, u32[]{:S(2)}) collective-permute-start(bf16[256,512]{0,1:T(8,128)(2,1)S(1)} %collective-permute-done.7), channel_id=1, source_target_pairs={{0,64},{8,72},{16,80},{24,88},{32,96},{40,104},{48,112},{56,120},{... | collective-permute-start | bytes 786440 | tf_op jit(solution)/shard_map/ppermute | solution.py:48
  870.4 12.1 %copy-start.8 = (f32[2,1,512]{2,1,0:T(1,128)S(1)}, f32[2,1,512]{2,1,0:T(1,128)}, u32[]{:S(2)}) copy-start(f32[2,1,512]{2,1,0:T(1,128)} %convert_element_type.154) | copy-start | bytes 12292
  882.8 6.8 copy-start.1
  (7 other events, 23.0 us)
Sparse Core Ops, SparseCore 0:
  9.7 75.4 all-gather.7
  130.3 31.7 all-gather.13
  163.8 22.4 all-gather.9
  187.8 19.0 all-gather.15
  385.7 14.9 all-gather.11
